TPU v7x, 32 devices: a whole 2x2x4 slice. The times are simulated.
32 devices in a mesh: sp: 8 (over z, y), tp: 4 (over x, core).
Axes of the slice: x: 2, y: 2, z: 4, core: 2. Of those that a mesh axis runs over, the one named last changes fastest.
Arguments:
- resid: bfloat16 [2048, 2048], P(('sp', 'tp')), may hold values from -0.21875 to 0.21875
- query_a: bfloat16 [2048, 1024], P('sp', 'tp'), may hold values from -6 to 6
- key_a: bfloat16 [2048, 256], P('sp', 'tp'), may hold values from -6 to 6
- value_a: bfloat16 [2048, 256], P('sp', 'tp'), may hold values from -6 to 6
- query_b: bfloat16 [2048, 1024], P('sp', 'tp'), may hold values from -6 to 6
- key_b: bfloat16 [2048, 512], P('sp', 'tp'), may hold values from -6 to 6
- value_b: bfloat16 [2048, 512], P('sp', 'tp'), may hold values from -6 to 6
- gain_qa: float32 [64], replicated, may hold values from 0.1 to 8
- gain_ka: float32 [64], replicated, may hold values from 0.1 to 8
- gain_qb: float32 [128], replicated, may hold values from 0.1 to 8
- gain_kb: float32 [128], replicated, may hold values from 0.1 to 8
- w_out_a: bfloat16 [1024, 2048], P('tp'), may hold values from -0.125 to 0.125
- w_out_b: bfloat16 [1024, 2048], P('tp'), may hold values from -0.125 to 0.125
- norm_gain: float32 [2048], replicated, may hold values from 0.1 to 1.9
- w_up: bfloat16 [2048, 8192], P('sp', 'tp'), may hold values from -0.125 to 0.125
- w_down: bfloat16 [8192, 2048], P('tp', 'sp'), may hold values from -0.0625 to 0.0625
Outputs:
- result: bfloat16 [2048, 2048], P(('sp', 'tp'))
All inputs are finite; a program needn't handle non-finite values.
Results may differ from a plain program's by a relative error of at most 0.02.
The roundings to bfloat16 on the way count: a program that leaves them out, or rounds other values in their place, can miss the bound.
Values may be sent and summed in bfloat16 or wider, within the bound.
No kernel may reach another device: no remote copies, remote signals or barrier semaphores. Data moves between devices by JAX's collectives and lax.ppermute only.
A program may use at most 128 MiB of HBM per device.

v0:
```python
import math

import jax
import jax.numpy as jnp
from jax import lax
from jax.sharding import PartitionSpec as P

GRID_W = 64


EPS = 1e-06


def norm_rope(values, gain, places):
    width = gain.shape[0]
    count = values.shape[0]
    flat = values.astype(jnp.float32).reshape(count, -1, width)
    flat = flat * lax.rsqrt(jnp.mean(flat * flat, axis=-1, keepdims=True) + EPS) * gain
    grid_rows = (places // GRID_W).astype(jnp.float32)
    grid_cols = (places % GRID_W).astype(jnp.float32)
    quarter = width // 4
    freqs = 10000.0 ** (-(2.0 * jnp.arange(quarter, dtype=jnp.float32)) / (width // 2))
    ang_r = grid_rows[:, None] * freqs
    ang_c = grid_cols[:, None] * freqs
    angles = jnp.concatenate([ang_r, ang_r, ang_c, ang_c], axis=-1)
    one, two, three, four = jnp.split(flat, 4, axis=-1)
    turned = jnp.concatenate([-two, one, -four, three], axis=-1)
    return (flat * jnp.cos(angles)[:, None, :] + turned * jnp.sin(angles)[:, None, :]).astype(
        jnp.bfloat16
    )


def fold_block(state, queries, key_block, value_block, scale):
    running, total, accum = state
    scores = (
        jnp.einsum("rkgd,pkd->kgrp", queries, key_block, preferred_element_type=jnp.float32) * scale
    )
    newest = jnp.maximum(running, jnp.max(scores, axis=-1))
    factor = jnp.exp(running - newest)
    expo = jnp.exp(scores - newest[..., None])
    total = total * factor + jnp.sum(expo, axis=-1)
    accum = accum * factor[..., None] + jnp.einsum(
        "kgrp,pkd->kgrd", expo.astype(jnp.bfloat16), value_block, preferred_element_type=jnp.float32
    )
    return (newest, total, accum)


def sweep_keys(state, queries, key_piece, value_piece, scale):
    length = key_piece.shape[0]
    block = math.gcd(length, 2048)
    blocks = length // block
    if blocks == 1:
        return fold_block(state, queries, key_piece, value_piece, scale)
    key_blocks = key_piece.reshape((blocks, block) + key_piece.shape[1:])
    value_blocks = value_piece.reshape((blocks, block) + value_piece.shape[1:])

    def advance(carry, pair):
        return (fold_block(carry, queries, pair[0], pair[1], scale), None)

    state, unused = lax.scan(advance, state, (key_blocks, value_blocks))
    return state


def start_state(queries):
    shape = (queries.shape[1], queries.shape[2], queries.shape[0])
    return (
        jnp.full(shape, -1e30, jnp.float32),
        jnp.zeros(shape, jnp.float32),
        jnp.zeros(shape + (queries.shape[3],), jnp.float32),
    )


def finish(state):
    running, total, accum = state
    outputs = accum / total[..., None]
    count = outputs.shape[2]
    return jnp.transpose(outputs, (2, 0, 1, 3)).reshape(count, -1).astype(jnp.bfloat16)


def local(
    resid,
    query_a,
    key_a,
    value_a,
    query_b,
    key_b,
    value_b,
    gain_qa,
    gain_ka,
    gain_qb,
    gain_kb,
    w_out_a,
    w_out_b,
    norm_gain,
    w_up,
    w_down,
):
    count = query_a.shape[0]
    width_a = gain_qa.shape[0]
    width_b = gain_qb.shape[0]
    places = lax.axis_index("sp") * count + jnp.arange(count, dtype=jnp.int32)
    keys_a = norm_rope(key_a, gain_ka, places)
    keys_b = norm_rope(key_b, gain_kb, places)
    heads_kv_a = keys_a.shape[1]
    heads_kv_b = keys_b.shape[1]
    queries_a = norm_rope(query_a, gain_qa, places)
    queries_b = norm_rope(query_b, gain_qb, places)
    queries_a = queries_a.reshape(count, heads_kv_a, queries_a.shape[1] // heads_kv_a, width_a)
    queries_b = queries_b.reshape(count, heads_kv_b, queries_b.shape[1] // heads_kv_b, width_b)
    values_a = value_a.reshape(count, heads_kv_a, width_a)
    values_b = value_b.reshape(count, heads_kv_b, width_b)
    state_a = sweep_keys(
        start_state(queries_a),
        queries_a,
        lax.all_gather(keys_a, "sp", axis=0, tiled=True),
        lax.all_gather(values_a, "sp", axis=0, tiled=True),
        width_a ** (-0.5),
    )
    state_b = sweep_keys(
        start_state(queries_b),
        queries_b,
        lax.all_gather(keys_b, "sp", axis=0, tiled=True),
        lax.all_gather(values_b, "sp", axis=0, tiled=True),
        width_b ** (-0.5),
    )
    attn_a = finish(state_a)
    attn_b = finish(state_b)
    rows_a, rows_b = (
        lax.all_to_all(attn_a, "tp", split_axis=0, concat_axis=1, tiled=True),
        lax.all_to_all(attn_b, "tp", split_axis=0, concat_axis=1, tiled=True),
    )
    whole_a, whole_b = (
        lax.all_gather(w_out_a, "tp", axis=0, tiled=True),
        lax.all_gather(w_out_b, "tp", axis=0, tiled=True),
    )
    proj = jnp.dot(rows_a, whole_a, preferred_element_type=jnp.float32) + jnp.dot(
        rows_b, whole_b, preferred_element_type=jnp.float32
    )
    mid = (resid.astype(jnp.float32) + proj).astype(jnp.bfloat16)
    midf = mid.astype(jnp.float32)
    normed = (
        midf * lax.rsqrt(jnp.mean(midf * midf, axis=-1, keepdims=True) + EPS) * norm_gain
    ).astype(jnp.bfloat16)
    up_whole, down_whole = (
        lax.all_gather(w_up, "sp", axis=0, tiled=True),
        lax.all_gather(w_down, "sp", axis=1, tiled=True),
    )
    hidden = jnp.square(
        jax.nn.relu(
            jnp.dot(
                lax.all_gather(normed, "tp", axis=0, tiled=True),
                up_whole,
                preferred_element_type=jnp.float32,
            )
        )
    ).astype(jnp.bfloat16)
    mixed = lax.psum_scatter(
        jnp.dot(hidden, down_whole, preferred_element_type=jnp.float32).astype(jnp.bfloat16),
        "tp",
        scatter_dimension=0,
        tiled=True,
    ).astype(jnp.float32)
    return (midf + mixed).astype(jnp.bfloat16)


def solution(mesh):
    return jax.shard_map(
        local,
        mesh=mesh,
        in_specs=(
            P(("sp", "tp"), None),
            P("sp", "tp"),
            P("sp", "tp"),
            P("sp", "tp"),
            P("sp", "tp"),
            P("sp", "tp"),
            P("sp", "tp"),
            P(),
            P(),
            P(),
            P(),
            P("tp", None),
            P("tp", None),
            P(),
            P("sp", "tp"),
            P("tp", "sp"),
        ),
        out_specs=P(("sp", "tp"), None),
        check_vma=False,
    )
```

profile of v0, /device:TPU:0, one launch (start us, length us, event | category | flops | bytes accessed | tf_op | source)
XLA Modules:
  0.0 480.9 jit_solution(12184441608509386701)
XLA Ops:
  6.5 0.7 all-gather.10.cloned.1.call-update
  7.3 0.0 all-gather.12.cloned.1.call-start
  7.3 0.7 all-gather.12.cloned.1.call-update
  8.1 1.0 fusion.53
  9.0 0.9 fusion.55
  10.0 0.2 fusion.63
  10.1 0.0 copy-start.1
  10.2 1.1 reshape.505
  11.3 0.3 multiply_reduce_fusion.1
  11.7 0.3 multiply_multiply_fusion
  12.0 0.9 slice_negate_fusion.1
  12.9 0.1 broadcast_multiply_fusion.1
  13.0 0.6 fusion.58
  13.7 33.2 %all-gather.2 = bf16[2048,128]{1,0:T(8,128)(2,1)S(1)} all-gather(bf16[256,128]{1,0:T(8,128)(2,1)S(1)} %get-tuple-element.5), channel_id=4, replica_groups=mesh['sp'=8,'tp'=4] {'sp'}, dimensions={0}, use_global_device_ids=true | all-gather | bytes 589824 | tf_op jit(solution)/shard_map/all_gather | solution.py:122
  46.9 0.9 maximum_multiply_fusion.1
  47.8 0.1 mul.427
  47.9 0.3 mul.420
  48.2 0.0 copy-start.5
  48.2 0.8 bitcast_reduce_fusion.1
  49.0 0.7 fusion.7
  49.7 0.0 copy-start.4
  49.7 0.0 copy-start.10
  49.7 0.0 copy-start.2
  49.7 0.0 copy-start.9
  49.8 31.4 %all-gather.3 = bf16[2048,128]{1,0:T(8,128)(2,1)S(1)} all-gather(bf16[256,128]{1,0:T(8,128)(2,1)S(1)} %copy-done.5), channel_id=5, replica_groups=mesh['sp'=8,'tp'=4] {'sp'}, dimensions={0}, use_global_device_ids=true | all-gather | bytes 589824 | tf_op jit(solution)/shard_map/all_gather | solution.py:123
  81.2 0.9 fusion.31
  82.1 0.1 copy.48
  82.2 0.7 convert_element_type.140
  83.0 3.3 all-to-all-start.1
  86.3 0.1 copy.40
  86.4 0.1 mul.388
  86.6 0.1 broadcast_multiply_fusion.3
  86.7 0.1 fusion.66
  86.8 0.1 fusion.69
  87.0 0.1 multiply_multiply_fusion.1
  87.1 0.1 fusion.49
  87.2 30.7 %all-gather = bf16[2048,64]{0,1:T(8,128)(2,1)S(1)} all-gather(bf16[256,64]{0,1:T(8,128)(2,1)S(1)} %get-tuple-element.26), channel_id=2, replica_groups=mesh['sp'=8,'tp'=4] {'sp'}, dimensions={0}, use_global_device_ids=true | all-gather | bytes 294912 | tf_op jit(solution)/shard_map/all_gather | solution.py:115
  118.0 30.9 %all-gather.1 = bf16[2048,64]{0,1:T(8,128)(2,1)S(1)} all-gather(bf16[256,64]{0,1:T(8,128)(2,1)S(1)} %copy-done.6), channel_id=3, replica_groups=mesh['sp'=8,'tp'=4] {'sp'}, dimensions={0}, use_global_device_ids=true | all-gather | bytes 294912 | tf_op jit(solution)/shard_map/all_gather | solution.py:116
  148.9 1.3 bitcast_reduce_fusion
  150.2 1.4 fusion.1
  151.6 1.5 fusion.40
  153.1 0.2 reshape.521
  153.3 0.8 copy.52
  154.1 3.3 all-to-all-start
  157.5 0.0 all-gather.14.cloned.1.call-start
  157.5 4.5 all-to-all-done
  162.1 0.0 all-gather.10.cloned.1.call-done
  162.1 3.0 fusion.86
  165.2 0.0 all-gather.12.cloned.1.call-done
  165.2 3.2 multiply_reduce_fusion
  168.4 0.8 multiply_convert_fusion
  169.2 0.0 all-gather.14.cloned.1.call-update
  169.3 0.0 all-gather.16.cloned.1.call-start
  169.3 0.5 all-gather.16.cloned.1.call-update
  169.8 0.0 all-gather.18.cloned.1.call-start
  169.9 0.5 all-gather.18.cloned.1.call-update
  170.4 0.0 reduce-scatter.2.cloned.1.call-start
  170.5 15.7 %all-gather.14.cloned.1.call-done = bf16[256,2048]{1,0:T(8,128)(2,1)} async-done(((bf16[64,2048]{1,0:T(8,128)(2,1)}), bf16[256,2048]{1,0:T(8,128)(2,1)}) %all-gather.14.cloned.1.call-update) | async-done | bytes 1048592 | tf_op jit(solution)/shard_map/all_gather | solution.py:151
  186.2 126.5 %all-gather.16.cloned.1.call-done = bf16[2048,2048]{1,0:T(8,128)(2,1)} async-done(((bf16[256,2048]{1,0:T(8,128)(2,1)}), bf16[2048,2048]{1,0:T(8,128)(2,1)}) %all-gather.16.cloned.1.call-update) | async-done | bytes 8388624 | tf_op jit(solution)/shard_map/all_gather | solution.py:145
  312.7 125.0 %all-gather.18.cloned.1.call-done = bf16[2048,2048]{1,0:T(8,128)(2,1)} async-done(((bf16[2048,256]{1,0:T(8,128)(2,1)}), bf16[2048,2048]{1,0:T(8,128)(2,1)}) %all-gather.18.cloned.1.call-update) | async-done | bytes 8388624 | tf_op jit(solution)/shard_map/all_gather | solution.py:146
  437.7 11.5 %convolution_convert_fusion = bf16[256,2048]{1,0:T(8,128)(2,1)} fusion(bf16[2048,2048]{1,0:T(8,128)(2,1)} %all-gather.18.cloned.1.call-done, bf16[256,2048]{1,0:T(8,128)(2,1)} %all-gather.14.cloned.1.call-done, bf16[2048,2048]{1,0:T(8,128)(2,1)} %all-gather.16.cloned.1.call-done), kind=kOutput, calls=%fused_computation.15 | convolution fusion | flops 4297064448 | bytes 18874368 | tf_op jit(solution)/shard_map/dot_general | solution.py:158
  449.2 0.0 reduce-scatter.2.cloned.1.call-update
  449.3 23.1 %reduce-scatter.2.cloned.1.call-done = bf16[64,2048]{1,0:T(8,128)(2,1)} async-done(((bf16[256,2048]{1,0:T(8,128)(2,1)}), bf16[64,2048]{1,0:T(8,128)(2,1)}) %reduce-scatter.2.cloned.1.call-update) | async-done | bytes 262160 | tf_op jit(solution)/shard_map/reduce_scatter | solution.py:157
  472.4 1.7 add_convert_fusion
  (41 shorter events, 0.3 us)
Async XLA Ops:
  6.5 6.5 %copy-start = (bf16[256,128]{1,0:T(8,128)(2,1)S(1)}, bf16[256,128]{1,0:T(8,128)(2,1)}, u32[]{:S(2)}) copy-start(bf16[256,128]{1,0:T(8,128)(2,1)} %param.21) | copy-start | bytes 196612
  6.5 6.5 %copy-start.8 = (f32[128]{0:T(128)S(1)}, f32[128]{0:T(128)}, u32[]{:S(2)}) copy-start(f32[128]{0:T(128)} %param.26) | copy-start | bytes 1540
  6.5 5.1 %copy-start.11 = (f32[128]{0:T(128)S(1)}, f32[128]{0:T(128)}, u32[]{:S(2)}) copy-start(f32[128]{0:T(128)} %param.25) | copy-start | bytes 1540
  6.5 155.6 %all-gather.10.cloned.1.call-start = ((), (), s32[]{:S(2)}) async-start(), calls=%async_computation.3 | async-start | bytes 5242880 | tf_op jit(solution)/shard_map/all_gather | solution.py:133
  7.3 157.9 %all-gather.12.cloned.1.call-start = ((), (), s32[]{:S(2)}) async-start(), calls=%async_computation.4 | async-start | bytes 5242880 | tf_op jit(solution)/shard_map/all_gather | solution.py:134
  10.1 38.1 %copy-start.1 = (bf16[256,256]{1,0:T(8,128)(2,1)S(1)}, bf16[256,256]{1,0:T(8,128)(2,1)}, u32[]{:S(2)}) copy-start(bf16[256,256]{1,0:T(8,128)(2,1)} %param.20) | copy-start | bytes 393220
  48.2 1.5 copy-start.5
  49.7 36.6 %copy-start.4 = (bf16[256,256]{1,0:T(8,128)(2,1)S(1)}, bf16[256,256]{1,0:T(8,128)(2,1)}, u32[]{:S(2)}) copy-start(bf16[256,256]{1,0:T(8,128)(2,1)} %param.17) | copy-start | bytes 393220
  49.7 36.7 %copy-start.10 = (f32[64]{0:T(128)S(1)}, f32[64]{0:T(128)}, u32[]{:S(2)}) copy-start(f32[64]{0:T(128)} %param.23) | copy-start | bytes 772
  49.7 36.8 %copy-start.2 = (bf16[256,64]{0,1:T(8,128)(2,1)S(1)}, bf16[256,64]{0,1:T(8,128)(2,1)}, u32[]{:S(2)}) copy-start(bf16[256,64]{0,1:T(8,128)(2,1)} %param.18) | copy-start | bytes 98308
  49.7 37.0 %copy-start.9 = (f32[64]{0:T(128)S(1)}, f32[64]{0:T(128)}, u32[]{:S(2)}) copy-start(f32[64]{0:T(128)} %param.24) | copy-start | bytes 772
  81.2 36.8 %copy-start.6 = (bf16[256,64]{0,1:T(8,128)(2,1)S(1)}, bf16[256,64]{0,1:T(8,128)(2,1)}, u32[]{:S(2)}) copy-start(bf16[256,64]{0,1:T(8,128)(2,1)} %param.19) | copy-start | bytes 98308
  83.0 71.1 %all-to-all-start.1 = ((bf16[4,64,256]{2,1,0:T(8,128)(2,1)}), bf16[4,64,256]{2,1,0:T(8,128)(2,1)S(1)}, u32[]{:S(2)}, u32[]{:S(2)}) async-start(bf16[4,64,256]{2,1,0:T(8,128)(2,1)} %convert_element_type.140), calls=%async_computation.1 | async-start | bytes 262144 | tf_op jit(solution)/shard_map/all_to_all | solution.py:130
  153.1 12.1 %copy-start.3 = (bf16[64,2048]{1,0:T(8,128)(2,1)S(1)}, bf16[64,2048]{1,0:T(8,128)(2,1)}, u32[]{:S(2)}) copy-start(bf16[64,2048]{1,0:T(8,128)(2,1)} %param.16) | copy-start | bytes 786436
  154.1 7.9 %all-to-all-start = ((bf16[4,64,256]{2,1,0:T(8,128)(2,1)}), bf16[4,64,256]{2,1,0:T(8,128)(2,1)S(1)}, u32[]{:S(2)}, u32[]{:S(2)}) async-start(bf16[4,64,256]{2,1,0:T(8,128)(2,1)} %copy.52), calls=%async_computation | async-start | bytes 262144 | tf_op jit(solution)/shard_map/all_to_all | solution.py:129
  157.5 28.7 %all-gather.14.cloned.1.call-start = ((), (), s32[]{:S(2)}) async-start(), calls=%async_computation.5 | async-start | bytes 1310720 | tf_op jit(solution)/shard_map/all_gather | solution.py:151
  162.1 6.3 %copy-start.7 = (f32[2048]{0:T(1024)S(1)}, f32[2048]{0:T(1024)}, u32[]{:S(2)}) copy-start(f32[2048]{0:T(1024)} %param.29) | copy-start | bytes 24580
  169.3 143.4 %all-gather.16.cloned.1.call-start = ((), (), s32[]{:S(2)}) async-start(), calls=%async_computation.6 | async-start | bytes 9437184 | tf_op jit(solution)/shard_map/all_gather | solution.py:145
  169.8 267.9 %all-gather.18.cloned.1.call-start = ((), (), s32[]{:S(2)}) async-start(), calls=%async_computation.7 | async-start | bytes 9437184 | tf_op jit(solution)/shard_map/all_gather | solution.py:146
  170.4 301.9 %reduce-scatter.2.cloned.1.call-start = ((), (), s32[]{:S(2)}) async-start(), calls=%async_computation.8 | async-start | bytes 1310720 | tf_op jit(solution)/shard_map/reduce_scatter | solution.py:157
Sparse Core Ops, SparseCore 0:
  8.9 37.1 all-gather.9
  47.7 34.4 all-gather.11
  169.4 16.7 all-gather.13
  188.1 124.4 all-gather.15
  314.6 123.1 all-gather.17
  449.4 22.9 reduce-scatter.1
where the time goes:
time: 481 us
  waiting for transfers between devices  297 us (62%)
  blocking collectives  126 us (26%)
  matrix products  22.3 us (5%)
  between operations  13.9 us (3%)
  other arithmetic  10.6 us (2%)
  starting transfers between devices  6.86 us (1%)
    all_gather x1, waiting for transfers between devices, local(): lax.all_gather(w_up, 'sp', axis=0, tiled=True)  126 us
    all_gather x1, waiting for transfers between devices, local(): lax.all_gather(w_down, 'sp', axis=1, tiled=True)  125 us
    all_gather x1, blocking collectives, local(): lax.all_gather(keys_b, 'sp', axis=0, tiled=True)  33.2 us
    all_gather x1, blocking collectives, local(): lax.all_gather(values_b, 'sp', axis=0, tiled=True)  31.4 us
    all_gather x1, blocking collectives, local(): lax.all_gather(values_a, 'sp', axis=0, tiled=True)  30.9 us
    all_gather x1, blocking collectives, local(): lax.all_gather(keys_a, 'sp', axis=0, tiled=True)  30.7 us
    reduce_scatter x1, waiting for transfers between devices, local(): lax.psum_scatter(jnp.dot(hidden, down_whole, preferred_element_type=jnp.f...  23.1 us
    all_gather x1, waiting for transfers between devices, local(): lax.all_gather(normed, 'tp', axis=0, tiled=True)  15.7 us
  transfers between devices with their start and end apart: 8, of which 5 were waited for; matrix products, arithmetic and copies ran while one was open for 4% of the time, Pallas kernels for 0%

commit v1 on v0

v1 whole, which is shorter than its diff:
```python
import math

import jax
import jax.numpy as jnp
from jax import lax
from jax.sharding import PartitionSpec as P

GRID_W = 64
EPS = 1e-06


def norm_rope(values, gain, places):
    width = gain.shape[0]
    count = values.shape[0]
    flat = values.astype(jnp.float32).reshape(count, -1, width)
    flat = flat * lax.rsqrt(jnp.mean(flat * flat, axis=-1, keepdims=True) + EPS) * gain
    grid_rows = (places // GRID_W).astype(jnp.float32)
    grid_cols = (places % GRID_W).astype(jnp.float32)
    quarter = width // 4
    freqs = 10000.0 ** (-(2.0 * jnp.arange(quarter, dtype=jnp.float32)) / (width // 2))
    ang_r = grid_rows[:, None] * freqs
    ang_c = grid_cols[:, None] * freqs
    angles = jnp.concatenate([ang_r, ang_r, ang_c, ang_c], axis=-1)
    one, two, three, four = jnp.split(flat, 4, axis=-1)
    turned = jnp.concatenate([-two, one, -four, three], axis=-1)
    return (flat * jnp.cos(angles)[:, None, :] + turned * jnp.sin(angles)[:, None, :]).astype(
        jnp.bfloat16
    )


def attend(queries, keys, values, scale):
    scores = (
        jnp.einsum("rkgd,pkd->kgrp", queries, keys, preferred_element_type=jnp.float32) * scale
    )
    top = jnp.max(scores, axis=-1, keepdims=True)
    expo = jnp.exp(scores - top)
    total = jnp.sum(expo, axis=-1)
    accum = jnp.einsum(
        "kgrp,pkd->kgrd",
        expo.astype(jnp.bfloat16),
        values,
        preferred_element_type=jnp.float32,
    )
    outputs = accum / total[..., None]
    return jnp.transpose(outputs, (2, 0, 1, 3)).reshape(queries.shape[0], -1).astype(jnp.bfloat16)


def make_local(sp, tp):
    low, core = 2, 2
    high, wide = sp // low, tp // core
    assert high * low == sp and wide * core == tp and wide == 2

    def over_high(value, step):
        pairs = [
            (h * low + l, ((h + step) % high) * low + l) for h in range(high) for l in range(low)
        ]
        return lax.ppermute(value, "sp", pairs)

    def over_low(value):
        return lax.ppermute(value, "sp", [(i, i ^ 1) for i in range(sp)])

    def over_wide(value):
        return lax.ppermute(value, "tp", [(i, (i + core) % tp) for i in range(tp)])

    def over_core(value):
        return lax.ppermute(value, "tp", [(i, i ^ 1) for i in range(tp)])

    high_groups = [[h * low + l for h in range(high)] for l in range(low)]

    def spread(piece):
        half = piece.shape[0] // 2
        by_low = over_low(piece)
        by_wide = over_wide(piece)
        across = jnp.concatenate([over_wide(by_low[:half]), over_low(by_wide[half:])], axis=0)
        mine = [[piece, by_wide], [by_low, across]]
        return [[[one, over_core(one)] for one in row] for row in mine]

    def local(
        resid,
        query_a,
        key_a,
        value_a,
        query_b,
        key_b,
        value_b,
        gain_qa,
        gain_ka,
        gain_qb,
        gain_kb,
        w_out_a,
        w_out_b,
        norm_gain,
        w_up,
        w_down,
    ):
        count = query_a.shape[0]
        width_a = gain_qa.shape[0]
        width_b = gain_qb.shape[0]
        model = resid.shape[1]
        s_index = lax.axis_index("sp")
        t_index = lax.axis_index("tp")
        l_index = s_index % low
        c_index = t_index % core
        x_index = t_index // core
        places = s_index * count + jnp.arange(count, dtype=jnp.int32)

        keys_a = norm_rope(key_a, gain_ka, places).reshape(count, -1)
        keys_b = norm_rope(key_b, gain_kb, places).reshape(count, -1)
        packed = jnp.concatenate([keys_b, value_b, keys_a, value_a], axis=1)
        blocks = [packed] + [over_high(packed, d) for d in range(1, high)]
        blocks = blocks + [over_low(block) for block in blocks]
        every = jnp.concatenate(blocks, axis=0)
        n_b, n_a = keys_b.shape[1], keys_a.shape[1]
        all_kb = every[:, :n_b].reshape(-1, n_b // width_b, width_b)
        all_vb = every[:, n_b : 2 * n_b].reshape(-1, n_b // width_b, width_b)
        all_ka = every[:, 2 * n_b : 2 * n_b + n_a].reshape(-1, n_a // width_a, width_a)
        all_va = every[:, 2 * n_b + n_a :].reshape(-1, n_a // width_a, width_a)

        queries_a = norm_rope(query_a, gain_qa, places)
        queries_b = norm_rope(query_b, gain_qb, places)
        kv_a, kv_b = n_a // width_a, n_b // width_b
        queries_a = queries_a.reshape(count, kv_a, -1, width_a)
        queries_b = queries_b.reshape(count, kv_b, -1, width_b)
        attn_a = attend(queries_a, all_ka, all_va, width_a ** (-0.5))
        attn_b = attend(queries_b, all_kb, all_vb, width_b ** (-0.5))

        attn = jnp.concatenate([attn_a, attn_b], axis=1)
        rows = count // tp
        attn = attn.reshape(wide, core, rows, -1)
        kept = lax.dynamic_index_in_dim(attn, c_index, 1, keepdims=False)
        sent = lax.dynamic_index_in_dim(attn, 1 - c_index, 1, keepdims=False)
        kept = kept.reshape(wide * rows, -1)
        came = over_core(sent.reshape(wide * rows, -1))
        w_out = jnp.concatenate([w_out_a, w_out_b], axis=0)
        w_out_other = over_core(w_out)
        part = jnp.dot(kept, w_out, preferred_element_type=jnp.float32) + jnp.dot(
            came, w_out_other, preferred_element_type=jnp.float32
        )
        part = part.reshape(wide, rows, model)
        part_kept = lax.dynamic_index_in_dim(part, x_index, 0, keepdims=False)
        part_sent = lax.dynamic_index_in_dim(part, 1 - x_index, 0, keepdims=False)
        part_came = over_wide(part_sent.astype(jnp.bfloat16)).astype(jnp.float32)
        mid = (resid.astype(jnp.float32) + (part_kept + part_came)).astype(jnp.bfloat16)
        midf = mid.astype(jnp.float32)
        normed = (
            midf * lax.rsqrt(jnp.mean(midf * midf, axis=-1, keepdims=True) + EPS) * norm_gain
        ).astype(jnp.bfloat16)

        block = w_up.shape[0]
        split = normed.reshape(rows, high, low, block)
        own = lax.dynamic_index_in_dim(split, l_index, 2, keepdims=False)
        other = lax.dynamic_index_in_dim(split, 1 - l_index, 2, keepdims=False)
        normed = jnp.concatenate([own.reshape(rows, -1), other.reshape(rows, -1)], axis=1)
        gathered = jnp.concatenate(
            [normed] + [over_high(normed, d) for d in range(1, high)], axis=0
        )

        up_piece = lax.all_to_all(
            w_up, "sp", split_axis=1, concat_axis=0, tiled=True, axis_index_groups=high_groups
        )
        down_piece = lax.all_to_all(
            w_down, "sp", split_axis=0, concat_axis=1, tiled=True, axis_index_groups=high_groups
        )
        ups = spread(up_piece)
        downs = spread(down_piece)

        inner = up_piece.shape[0]
        outs = [0.0, 0.0]
        for x in range(wide):
            for c in range(core):
                pre = jnp.dot(
                    gathered[:, :inner], ups[0][x][c], preferred_element_type=jnp.float32
                ) + jnp.dot(gathered[:, inner:], ups[1][x][c], preferred_element_type=jnp.float32)
                hidden = jnp.square(jax.nn.relu(pre)).astype(jnp.bfloat16)
                for l in range(low):
                    outs[l] = outs[l] + jnp.dot(
                        hidden, downs[l][x][c], preferred_element_type=jnp.float32
                    )
        out = jnp.concatenate(outs, axis=1)
        mixed = out[:rows]
        for d in range(1, high):
            mixed = mixed + over_high(
                out[d * rows : (d + 1) * rows].astype(jnp.bfloat16), -d
            ).astype(jnp.float32)
        first, second = mixed[:, :inner], mixed[:, inner:]
        even = jnp.where(l_index == 0, first, second).reshape(rows, high, 1, block)
        odd = jnp.where(l_index == 0, second, first).reshape(rows, high, 1, block)
        mixed = jnp.concatenate([even, odd], axis=2).reshape(rows, model)
        return (midf + mixed).astype(jnp.bfloat16)

    return local


def solution(mesh):
    return jax.shard_map(
        make_local(mesh.shape["sp"], mesh.shape["tp"]),
        mesh=mesh,
        in_specs=(
            P(("sp", "tp"), None),
            P("sp", "tp"),
            P("sp", "tp"),
            P("sp", "tp"),
            P("sp", "tp"),
            P("sp", "tp"),
            P("sp", "tp"),
            P(),
            P(),
            P(),
            P(),
            P("tp", None),
            P("tp", None),
            P(),
            P("sp", "tp"),
            P("tp", "sp"),
        ),
        out_specs=P(("sp", "tp"), None),
        check_vma=False,
    )
```

time: 481 us -> 196 us (0.41)
  waiting for transfers between devices: 297 us -> 81.6 us
  blocking collectives: 126 us -> 0 us
  local copies, waits for them, and re-layouts: 3.64 us -> 31.9 us
  starting transfers between devices: 6.86 us -> 33.9 us
  between operations: 13.9 us -> 0.73 us
  other arithmetic: 10.6 us -> 20.5 us
    all_gather x5 -> x0, waiting for transfers between devices: 267 us -> none  [the longest x1 126 us: local(): lax.all_gather(w_up, 'sp', axis=0, tiled=True)]
    all_gather x4 -> x0, blocking collectives: 126 us -> none  [the longest x1 33.2 us: local(): lax.all_gather(keys_b, 'sp', axis=0, tiled=True)]
    ppermute x0 -> x32, waiting for transfers between devices: none -> 70.5 us  [the longest x9 49.1 us: over_high(): return lax.ppermute(value, 'sp', pairs)]
    ppermute x0 -> x32, starting transfers between devices: none -> 25.4 us  [the longest x9 11 us: over_high(): return lax.ppermute(value, 'sp', pairs)]
    reduce_scatter x1 -> x0, waiting for transfers between devices: 23.1 us -> none  [local(): lax.psum_scatter(jnp.dot(hidden, down_whole, preferred_element_type=jnp.f...]
    unnamed x25 -> x38, local copies, waits for them, and re-layouts: 0.16 us -> 16.7 us
    all_to_all x2, waiting for transfers between devices: 4.55 us -> 11.1 us  [the longest x1 11.1 us: local(): lax.all_to_all(w_down, 'sp', split_axis=0, concat_axis=1, tiled=True, axi...]
    dot_general x7 -> x22, matrix products: 22.3 us -> 25.6 us  [the longest x2 6.93 us: attend(): jnp.einsum('kgrp,pkd->kgrd', expo.astype(jnp.bfloat16), values, preferred...]
  transfers between devices with their start and end apart: 8 -> 34, of which waited for: 5 -> 14; matrix products, arithmetic and copies ran while one was open for 4% -> 32% of each run, Pallas kernels for 0% -> 0%
where the time goes in v1:
time: 196 us; the launch traced here: 194 us
  waiting for transfers between devices  81.6 us (42%)
  starting transfers between devices  33.9 us (17%)
  local copies, waits for them, and re-layouts  31.9 us (16%)
  matrix products  25.6 us (13%)
  other arithmetic  20.5 us (10%)
    ppermute x9, waiting for transfers between devices, over_high(): return lax.ppermute(value, 'sp', pairs)  49.1 us
    unnamed x38, local copies, waits for them, and re-layouts  16.7 us
    ppermute x5, waiting for transfers between devices, over_wide(): return lax.ppermute(value, 'tp', [(i, (i + core) % tp) for i in range(tp)])  11.7 us
    all_to_all x1, waiting for transfers between devices, local(): lax.all_to_all(w_down, 'sp', split_axis=0, concat_axis=1, tiled=True, axi...  11.1 us
    ppermute x9, starting transfers between devices, over_high(): return lax.ppermute(value, 'sp', pairs)  11 us
    ppermute x8, waiting for transfers between devices, over_low(): return lax.ppermute(value, 'sp', [(i, i ^ 1) for i in range(sp)])  8.47 us
    ppermute x8, starting transfers between devices, over_low(): return lax.ppermute(value, 'sp', [(i, i ^ 1) for i in range(sp)])  7.36 us
    dot_general x2, matrix products, attend(): jnp.einsum('kgrp,pkd->kgrd', expo.astype(jnp.bfloat16), values, preferred...  6.93 us
  transfers between devices with their start and end apart: 34, of which 14 were waited for; matrix products, arithmetic and copies ran while one was open for 32% of the time, Pallas kernels for 0%

profile of v1, /device:TPU:0, one launch (start us, length us, event | category | flops | bytes accessed | tf_op | source)
XLA Modules:
  0.0 194.3 jit_solution(9170518797432142419)
XLA Ops:
  0.1 1.0 copy.82
  2.0 0.8 fusion.89
  2.8 0.8 fusion.91
  3.7 0.9 copy.83
  4.6 1.6 fusion.88
  6.2 1.6 fusion.94
  7.8 0.8 pad_maximum_fusion.3
  8.6 3.1 %collective-permute-start = (bf16[256,384]{0,1:T(8,128)(2,1)}, bf16[256,384]{0,1:T(8,128)(2,1)}, u32[]{:S(2)}, u32[]{:S(2)}) collective-permute-start(bf16[256,384]{0,1:T(8,128)(2,1)} %get-tuple-element.26), channel_id=1, source_target_pairs={{0,8},{4,12},{8,16},{12,20},{16,24},{20,28},{24,0},{28,4},{1,9},{5... | collective-permute-start | bytes 589832 | tf_op jit(solution)/shard_map/ppermute | solution.py:57
  11.6 2.6 %collective-permute-start.1 = (bf16[256,384]{0,1:T(8,128)(2,1)}, bf16[256,384]{0,1:T(8,128)(2,1)}, u32[]{:S(2)}, u32[]{:S(2)}) collective-permute-start(bf16[256,384]{0,1:T(8,128)(2,1)} %get-tuple-element.26), channel_id=1, source_target_pairs={{0,16},{4,20},{8,24},{12,28},{16,0},{20,4},{24,8},{28,12},{1,17},{... | collective-permute-start | bytes 589832 | tf_op jit(solution)/shard_map/ppermute | solution.py:57
  14.2 1.3 collective-permute-start.2
  15.6 1.5 collective-permute-start.3
  17.2 1.3 constant_dynamic-update-slice_fusion.8
  18.6 2.3 %copy.98 = bf16[256,2048]{0,1:T(8,128)(2,1)} copy(bf16[256,2048]{1,0:T(8,128)(2,1)} %param.30) | data formatting | bytes 2097152 | tf_op args[14]
  20.9 3.6 %all-to-all-start = ((bf16[256,4,512]{0,2,1:T(8,128)(2,1)}), bf16[256,4,512]{0,2,1:T(8,128)(2,1)S(1)}, u32[]{:S(2)}, u32[]{:S(2)}) async-start(bf16[256,4,512]{0,2,1:T(8,128)(2,1)} %bitcast.218), calls=%async_computation | async-start | bytes 2097152 | tf_op jit(solution)/shard_map/all_to_all | solution.py:158
  26.2 1.8 slice_negate_fusion.1
  28.0 1.0 copy.84
  29.2 2.8 %maximum_multiply_fusion.1 = f32[256,2,128]{2,1,0:T(2,128)} fusion(f32[256,2,32]{2,1,0:T(2,128)} %get-tuple-element.19, f32[256,2,32]{2,1,0:T(2,128)} %get-tuple-element.20, f32[256,2,32]{2,1,0:T(2,128)} %get-tuple-element.21, f32[256,2,32]{2,1,0:T(2,128)} %get-tuple-element.18, f32[256,128]{1,0:T(8,128)} %copy.90), kind=kLoop, calls=%fused_computation.97 | loop fusion | flops 262144 | bytes 655360 | tf_op jit(solution)/shard_map/mul | solution.py:26
  32.8 0.8 copy.89
  33.6 1.1 fusion.74
  35.3 1.5 collective-permute-start.5
  36.8 1.6 constant_dynamic-update-slice_fusion.6
  39.0 1.6 constant_dynamic-update-slice_fusion.5
  40.6 1.6 constant_dynamic-update-slice_fusion.4
  42.3 1.6 constant_dynamic-update-slice_fusion.3
  44.6 2.4 %collective-permute-done.5 = bf16[256,384]{0,1:T(8,128)(2,1)S(1)} collective-permute-done((bf16[256,384]{0,1:T(8,128)(2,1)}, bf16[256,384]{0,1:T(8,128)(2,1)S(1)}, u32[]{:S(2)}, u32[]{:S(2)}) %collective-permute-start.5) | collective-permute-done | bytes 196640 | tf_op jit(solution)/shard_map/ppermute | solution.py:60
  47.7 3.0 %collective-permute-done.6 = bf16[256,384]{0,1:T(8,128)(2,1)S(1)} collective-permute-done((bf16[256,384]{0,1:T(8,128)(2,1)}, bf16[256,384]{0,1:T(8,128)(2,1)S(1)}, u32[]{:S(2)}, u32[]{:S(2)}) %collective-permute-start.6) | collective-permute-done | bytes 196640 | tf_op jit(solution)/shard_map/ppermute | solution.py:60
  51.9 1.8 bitcast_reduce_fusion.1
  54.4 1.9 %fusion.35 = bf16[256,1,2,128]{3,0,2,1:T(8,128)(2,1)S(1)} fusion(f32[2048,256,2]{1,0,2:T(8,128)S(1)} %get-tuple-element.49, f32[2,256]{1,0:T(2,128)S(1)} %get-tuple-element.48, bf16[2048,384]{0,1:T(8,128)(2,1)} %constant_dynamic-update-slice_fusion, f32[2,256]{1,0:T(2,128)S(1)} %fusion.7), kind=kOutput, calls=%fused_computation.45 | convolution fusion | flops 271712256 | bytes 4853760 | tf_op jit(solution)/shard_map/kgrp,pkd->kgrd/dot_general | solution.py:38
  57.3 2.2 %bitcast_reduce_fusion = (f32[4,256]{1,0:T(4,128)S(1)}, f32[2048,256,4]{1,0,2:T(8,128)S(1)}) fusion(bf16[256,4,64]{0,2,1:T(8,128)(2,1)S(1)} %bitcast.229, bf16[2048,384]{0,1:T(8,128)(2,1)} %constant_dynamic-update-slice_fusion), kind=kOutput, calls=%fused_computation.1 | convolution fusion | flops 272628736 | bytes 8785920 | tf_op jit(solution)/shard_map/rkgd,pkd->kgrp/dot_general | solution.py:33
  59.5 3.3 %copy-done = f32[2048,256,4]{1,0,2:T(8,128)} copy-done((f32[2048,256,4]{1,0,2:T(8,128)}, f32[2048,256,4]{1,0,2:T(8,128)S(1)}, u32[]{:S(2)}) %copy-start) | copy-done | bytes 8388632
  62.8 1.4 fusion.1
  64.2 4.8 %all-to-all-start.1 = ((bf16[4,512,256]{2,1,0:T(8,128)(2,1)}), bf16[4,512,256]{2,1,0:T(8,128)(2,1)}, u32[]{:S(2)}, u32[]{:S(2)}) async-start(bf16[4,512,256]{2,1,0:T(8,128)(2,1)} %bitcast.227), calls=%async_computation.1 | async-start | bytes 2097152 | tf_op jit(solution)/shard_map/all_to_all | solution.py:161
  68.9 5.0 %fusion.44 = bf16[256,1,4,64]{0,3,2,1:T(8,128)(2,1)S(1)} fusion(f32[2048,256,4]{1,0,2:T(8,128)} %copy-done, f32[4,256]{1,0:T(4,128)S(1)} %get-tuple-element.46, bf16[2048,384]{0,1:T(8,128)(2,1)} %constant_dynamic-update-slice_fusion, f32[4,256]{1,0:T(4,128)S(1)} %fusion.1), kind=kOutput, calls=%fused_computation.48 | convolution fusion | flops 274857984 | bytes 8790016 | tf_op jit(solution)/shard_map/kgrp,pkd->kgrd/dot_general | solution.py:38
  74.3 0.9 fusion.83
  75.7 0.9 collective-permute-done.7
  76.6 2.0 %convolution_add_fusion = f32[128,2048]{1,0:T(8,128)S(1)} fusion(f32[128,2048]{1,0:T(8,128)S(1)} %fusion.108, bf16[128,512]{1,0:T(8,128)(2,1)S(1)} %collective-permute-done.7, bf16[512,2048]{1,0:T(8,128)(2,1)} %collective-permute-done.8), kind=kOutput, calls=%fused_computation.15 | convolution fusion | flops 268697600 | bytes 4325376 | tf_op jit(solution)/shard_map/dot_general | solution.py:136
  79.4 1.5 collective-permute-start.9
  80.9 1.3 copy.99
  83.2 11.1 %all-to-all-done.1 = bf16[4,512,256]{2,1,0:T(8,128)(2,1)} async-done(((bf16[4,512,256]{2,1,0:T(8,128)(2,1)}), bf16[4,512,256]{2,1,0:T(8,128)(2,1)}, u32[]{:S(2)}, u32[]{:S(2)}) %all-to-all-start.1) | async-done | bytes 1048608 | tf_op jit(solution)/shard_map/all_to_all | solution.py:161
  94.3 1.5 copy.100
  96.4 1.5 collective-permute-start.20
  97.9 1.2 fusion.47
  99.5 1.6 dynamic-slice_reduce_fusion
  101.2 9.0 %collective-permute-done.10 = bf16[64,2048]{1,0:T(8,128)(2,1)S(1)} collective-permute-done((bf16[64,2048]{1,0:T(8,128)(2,1)S(1)}, bf16[64,2048]{1,0:T(8,128)(2,1)S(1)}, u32[]{:S(2)}, u32[]{:S(2)}) %collective-permute-start.10) | collective-permute-done | bytes 262176 | tf_op jit(solution)/shard_map/ppermute | solution.py:57
  110.3 10.7 %collective-permute-done.11 = bf16[64,2048]{1,0:T(8,128)(2,1)S(1)} collective-permute-done((bf16[64,2048]{1,0:T(8,128)(2,1)S(1)}, bf16[64,2048]{1,0:T(8,128)(2,1)S(1)}, u32[]{:S(2)}, u32[]{:S(2)}) %collective-permute-start.11) | collective-permute-done | bytes 262176 | tf_op jit(solution)/shard_map/ppermute | solution.py:57
  121.8 7.5 %collective-permute-done.12 = bf16[64,2048]{1,0:T(8,128)(2,1)S(1)} collective-permute-done((bf16[64,2048]{1,0:T(8,128)(2,1)S(1)}, bf16[64,2048]{1,0:T(8,128)(2,1)S(1)}, u32[]{:S(2)}, u32[]{:S(2)}) %collective-permute-start.12) | collective-permute-done | bytes 262176 | tf_op jit(solution)/shard_map/ppermute | solution.py:57
  130.0 1.1 slice.79
  131.6 1.1 slice.80
  132.7 1.6 collective-permute-start.19
  134.4 1.6 collective-permute-start.26
  135.9 1.1 slice.82
  137.0 1.7 fusion.63
  138.7 1.7 fusion.28
  142.3 3.6 %collective-permute-done.18 = bf16[512,512]{1,0:T(8,128)(2,1)S(1)} collective-permute-done((bf16[512,512]{1,0:T(8,128)(2,1)S(1)}, bf16[512,512]{1,0:T(8,128)(2,1)S(1)}, u32[]{:S(2)}, u32[]{:S(2)}) %collective-permute-start.18) | collective-permute-done | bytes 524320 | tf_op jit(solution)/shard_map/ppermute | solution.py:63
  146.0 1.6 collective-permute-done.19
  148.1 8.1 %collective-permute-done.26 = bf16[256,1024]{0,1:T(8,128)(2,1)S(1)} collective-permute-done((bf16[256,1024]{0,1:T(8,128)(2,1)S(1)}, bf16[256,1024]{0,1:T(8,128)(2,1)S(1)}, u32[]{:S(2)}, u32[]{:S(2)}) %collective-permute-start.26) | collective-permute-done | bytes 524320 | tf_op jit(solution)/shard_map/ppermute | solution.py:63
  156.2 1.4 collective-permute-done.27
  157.6 1.7 fusion.26
  161.4 1.7 convolution_add_fusion.3
  166.0 2.1 %collective-permute-start.29 = (bf16[64,2048]{1,0:T(8,128)(2,1)S(1)}, bf16[64,2048]{1,0:T(8,128)(2,1)S(1)}, u32[]{:S(2)}, u32[]{:S(2)}) collective-permute-start(bf16[64,2048]{1,0:T(8,128)(2,1)S(1)} %get-tuple-element.11), channel_id=1, source_target_pairs={{0,24},{4,28},{8,0},{12,4},{16,8},{20,12},{24,16},{28,20},{1,25},{... | collective-permute-start | bytes 786440 | tf_op jit(solution)/shard_map/ppermute | solution.py:57
  168.2 1.1 collective-permute-start.31
  169.3 6.1 %collective-permute-done.29 = bf16[64,2048]{1,0:T(8,128)(2,1)S(1)} collective-permute-done((bf16[64,2048]{1,0:T(8,128)(2,1)S(1)}, bf16[64,2048]{1,0:T(8,128)(2,1)S(1)}, u32[]{:S(2)}, u32[]{:S(2)}) %collective-permute-start.29) | collective-permute-done | bytes 262176 | tf_op jit(solution)/shard_map/ppermute | solution.py:57
  175.4 15.7 %collective-permute-done.30 = bf16[64,2048]{1,0:T(8,128)(2,1)} collective-permute-done((bf16[64,2048]{1,0:T(8,128)(2,1)S(1)}, bf16[64,2048]{1,0:T(8,128)(2,1)}, u32[]{:S(2)}, u32[]{:S(2)}) %collective-permute-start.30) | collective-permute-done | bytes 262176 | tf_op jit(solution)/shard_map/ppermute | solution.py:57
  191.1 1.1 fusion.54
  (134 shorter events, 24.0 us)
Async XLA Ops:
  0.0 7.8 %copy-start.7 = (bf16[256,64]{0,1:T(8,128)(2,1)S(1)}, bf16[256,64]{0,1:T(8,128)(2,1)}, u32[]{:S(2)}) copy-start(bf16[256,64]{0,1:T(8,128)(2,1)} %param.19) | copy-start | bytes 98308
  0.0 17.1 %copy-start.1 = (bf16[256,2048]{1,0:T(8,128)(2,1)S(1)}, bf16[256,2048]{1,0:T(8,128)(2,1)}, u32[]{:S(2)}) copy-start(bf16[256,2048]{1,0:T(8,128)(2,1)} %param.27) | copy-start | bytes 3145732
  8.6 26.1 %collective-permute-start = (bf16[256,384]{0,1:T(8,128)(2,1)}, bf16[256,384]{0,1:T(8,128)(2,1)}, u32[]{:S(2)}, u32[]{:S(2)}) collective-permute-start(bf16[256,384]{0,1:T(8,128)(2,1)} %get-tuple-element.26), channel_id=1, source_target_pairs={{0,8},{4,12},{8,16},{12,20},{16,24},{20,28},{24,0},{28,4},{1,9},{5... | collective-permute-start | bytes 589832 | tf_op jit(solution)/shard_map/ppermute | solution.py:57
  11.6 23.7 %collective-permute-start.1 = (bf16[256,384]{0,1:T(8,128)(2,1)}, bf16[256,384]{0,1:T(8,128)(2,1)}, u32[]{:S(2)}, u32[]{:S(2)}) collective-permute-start(bf16[256,384]{0,1:T(8,128)(2,1)} %get-tuple-element.26), channel_id=1, source_target_pairs={{0,16},{4,20},{8,24},{12,28},{16,0},{20,4},{24,8},{28,12},{1,17},{... | collective-permute-start | bytes 589832 | tf_op jit(solution)/shard_map/ppermute | solution.py:57
  14.2 24.3 %collective-permute-start.2 = (bf16[256,384]{0,1:T(8,128)(2,1)}, bf16[256,384]{0,1:T(8,128)(2,1)}, u32[]{:S(2)}, u32[]{:S(2)}) collective-permute-start(bf16[256,384]{0,1:T(8,128)(2,1)} %get-tuple-element.26), channel_id=1, source_target_pairs={{0,24},{4,28},{8,0},{12,4},{16,8},{20,12},{24,16},{28,20},{1,25},{... | collective-permute-start | bytes 589832 | tf_op jit(solution)/shard_map/ppermute | solution.py:57
  15.6 26.7 %collective-permute-start.3 = (bf16[256,384]{0,1:T(8,128)(2,1)}, bf16[256,384]{0,1:T(8,128)(2,1)}, u32[]{:S(2)}, u32[]{:S(2)}) collective-permute-start(bf16[256,384]{0,1:T(8,128)(2,1)} %get-tuple-element.26), channel_id=1, source_target_pairs={{0,4},{4,0},{8,12},{12,8},{16,20},{20,16},{24,28},{28,24},{1,5},{5... | collective-permute-start | bytes 589832 | tf_op jit(solution)/shard_map/ppermute | solution.py:60
  18.5 6.8 %copy-start.3 = (bf16[256,256]{1,0:T(8,128)(2,1)S(1)}, bf16[256,256]{1,0:T(8,128)(2,1)}, u32[]{:S(2)}) copy-start(bf16[256,256]{1,0:T(8,128)(2,1)} %param.20) | copy-start | bytes 393220
  18.5 58.1 %collective-permute-start.8 = (bf16[512,2048]{1,0:T(8,128)(2,1)S(1)}, bf16[512,2048]{1,0:T(8,128)(2,1)}, u32[]{:S(2)}, u32[]{:S(2)}) collective-permute-start(bf16[512,2048]{1,0:T(8,128)(2,1)S(1)} %constant_dynamic-update-slice_fusion.8), channel_id=1, source_target_pairs={{0,1},{1,0},{2,3},{3,2},{4,5},{5,4},{6,7},{7,6},{8,9},{9,8},{10,11... | collective-permute-start | bytes 6291464 | tf_op jit(solution)/shard_map/ppermute | solution.py:66
  20.9 5.0 %copy-start.10 = (f32[128]{0:T(128)S(1)}, f32[128]{0:T(128)}, u32[]{:S(2)}) copy-start(f32[128]{0:T(128)} %param.25) | copy-start | bytes 1540
  20.9 43.3 %all-to-all-start = ((bf16[256,4,512]{0,2,1:T(8,128)(2,1)}), bf16[256,4,512]{0,2,1:T(8,128)(2,1)S(1)}, u32[]{:S(2)}, u32[]{:S(2)}) async-start(bf16[256,4,512]{0,2,1:T(8,128)(2,1)} %bitcast.218), calls=%async_computation | async-start | bytes 2097152 | tf_op jit(solution)/shard_map/all_to_all | solution.py:158
  25.5 3.6 %copy-start.9 = (f32[64]{0:T(128)S(1)}, f32[64]{0:T(128)}, u32[]{:S(2)}) copy-start(f32[64]{0:T(128)} %param.23) | copy-start | bytes 772
  28.0 4.8 %copy-start.5 = (f32[256,128]{0,1:T(8,128)S(1)}, f32[256,128]{0,1:T(8,128)}, u32[]{:S(2)}) copy-start(f32[256,128]{0,1:T(8,128)} %get-tuple-element.32) | copy-start | bytes 393220
  29.0 3.0 %copy-start.6 = (f32[256,64]{0,1:T(8,128)S(1)}, f32[256,64]{0,1:T(8,128)}, u32[]{:S(2)}) copy-start(f32[256,64]{0,1:T(8,128)} %get-tuple-element.40) | copy-start | bytes 196612
  33.6 17.8 %copy-start.4 = (f32[256,128]{1,0:T(8,128)S(1)}, f32[256,128]{1,0:T(8,128)}, u32[]{:S(2)}) copy-start(f32[256,128]{1,0:T(8,128)} %copy.89) | copy-start | bytes 393220
  33.6 18.3 %copy-start.2 = (f32[256,2,128]{2,1,0:T(2,128)S(1)}, f32[256,2,128]{2,1,0:T(2,128)}, u32[]{:S(2)}) copy-start(f32[256,2,128]{2,1,0:T(2,128)} %maximum_multiply_fusion.1) | copy-start | bytes 786436
  34.7 9.2 %collective-permute-start.4 = (bf16[256,384]{0,1:T(8,128)(2,1)}, bf16[256,384]{0,1:T(8,128)(2,1)S(1)}, u32[]{:S(2)}, u32[]{:S(2)}) collective-permute-start(bf16[256,384]{0,1:T(8,128)(2,1)} %collective-permute-done), channel_id=1, source_target_pairs={{0,4},{4,0},{8,12},{12,8},{16,20},{20,16},{24,28},{28,24},{1,5},{5... | collective-permute-start | bytes 589832 | tf_op jit(solution)/shard_map/ppermute | solution.py:60
  35.3 11.7 %collective-permute-start.5 = (bf16[256,384]{0,1:T(8,128)(2,1)}, bf16[256,384]{0,1:T(8,128)(2,1)S(1)}, u32[]{:S(2)}, u32[]{:S(2)}) collective-permute-start(bf16[256,384]{0,1:T(8,128)(2,1)} %collective-permute-done.1), channel_id=1, source_target_pairs={{0,4},{4,0},{8,12},{12,8},{16,20},{20,16},{24,28},{28,24},{1,5},{5... | collective-permute-start | bytes 589832 | tf_op jit(solution)/shard_map/ppermute | solution.py:60
  38.5 12.3 %collective-permute-start.6 = (bf16[256,384]{0,1:T(8,128)(2,1)}, bf16[256,384]{0,1:T(8,128)(2,1)S(1)}, u32[]{:S(2)}, u32[]{:S(2)}) collective-permute-start(bf16[256,384]{0,1:T(8,128)(2,1)} %collective-permute-done.2), channel_id=1, source_target_pairs={{0,4},{4,0},{8,12},{12,8},{16,20},{20,16},{24,28},{28,24},{1,5},{5... | collective-permute-start | bytes 589832 | tf_op jit(solution)/shard_map/ppermute | solution.py:60
  59.5 3.3 %copy-start = (f32[2048,256,4]{1,0,2:T(8,128)}, f32[2048,256,4]{1,0,2:T(8,128)S(1)}, u32[]{:S(2)}) copy-start(f32[2048,256,4]{1,0,2:T(8,128)S(1)} %get-tuple-element.47) | copy-start | bytes 25165828
  64.2 30.1 %all-to-all-start.1 = ((bf16[4,512,256]{2,1,0:T(8,128)(2,1)}), bf16[4,512,256]{2,1,0:T(8,128)(2,1)}, u32[]{:S(2)}, u32[]{:S(2)}) async-start(bf16[4,512,256]{2,1,0:T(8,128)(2,1)} %bitcast.227), calls=%async_computation.1 | async-start | bytes 2097152 | tf_op jit(solution)/shard_map/all_to_all | solution.py:161
  75.2 1.4 collective-permute-start.7
  79.4 18.5 %collective-permute-start.9 = (bf16[64,2048]{1,0:T(8,128)(2,1)}, bf16[64,2048]{1,0:T(8,128)(2,1)}, u32[]{:S(2)}, u32[]{:S(2)}) collective-permute-start(bf16[64,2048]{1,0:T(8,128)(2,1)} %fusion.70), channel_id=1, source_target_pairs={{0,2},{1,3},{2,0},{3,1},{4,6},{5,7},{6,4},{7,5},{8,10},{9,11},{10,... | collective-permute-start | bytes 786440 | tf_op jit(solution)/shard_map/ppermute | solution.py:63
  82.2 16.9 %copy-start.8 = (f32[2048]{0:T(1024)S(1)}, f32[2048]{0:T(1024)}, u32[]{:S(2)}) copy-start(f32[2048]{0:T(1024)} %param.29) | copy-start | bytes 24580
  82.2 47.2 %collective-permute-start.13 = (bf16[1024,512]{1,0:T(8,128)(2,1)}, bf16[1024,512]{1,0:T(8,128)(2,1)}, u32[]{:S(2)}, u32[]{:S(2)}) collective-permute-start(bf16[1024,512]{1,0:T(8,128)(2,1)} %bitcast.39), channel_id=1, source_target_pairs={{0,4},{4,0},{8,12},{12,8},{16,20},{20,16},{24,28},{28,24},{1,5},{5... | collective-permute-start | bytes 3145736 | tf_op jit(solution)/shard_map/ppermute | solution.py:60
  82.7 48.3 %collective-permute-start.17 = (bf16[1024,512]{1,0:T(8,128)(2,1)}, bf16[1024,512]{1,0:T(8,128)(2,1)}, u32[]{:S(2)}, u32[]{:S(2)}) collective-permute-start(bf16[1024,512]{1,0:T(8,128)(2,1)} %bitcast.39), channel_id=1, source_target_pairs={{0,2},{1,3},{2,0},{3,1},{4,6},{5,7},{6,4},{7,5},{8,10},{9,11},{10,... | collective-permute-start | bytes 3145736 | tf_op jit(solution)/shard_map/ppermute | solution.py:63
  95.8 36.9 %collective-permute-start.24 = (bf16[512,1024]{0,1:T(8,128)(2,1)S(1)}, bf16[512,1024]{0,1:T(8,128)(2,1)S(1)}, u32[]{:S(2)}, u32[]{:S(2)}) collective-permute-start(bf16[512,1024]{0,1:T(8,128)(2,1)S(1)} %bitcast.219), channel_id=1, source_target_pairs={{0,4},{4,0},{8,12},{12,8},{16,20},{20,16},{24,28},{28,24},{1,5},{5... | collective-permute-start | bytes 3145736 | tf_op jit(solution)/shard_map/ppermute | solution.py:60
  96.4 38.0 %collective-permute-start.20 = (bf16[512,1024]{0,1:T(8,128)(2,1)S(1)}, bf16[512,1024]{0,1:T(8,128)(2,1)}, u32[]{:S(2)}, u32[]{:S(2)}) collective-permute-start(bf16[512,1024]{0,1:T(8,128)(2,1)S(1)} %bitcast.220), channel_id=1, source_target_pairs={{0,2},{1,3},{2,0},{3,1},{4,6},{5,7},{6,4},{7,5},{8,10},{9,11},{10,... | collective-permute-start | bytes 3145736 | tf_op jit(solution)/shard_map/ppermute | solution.py:63
  101.2 9.1 %collective-permute-start.10 = (bf16[64,2048]{1,0:T(8,128)(2,1)S(1)}, bf16[64,2048]{1,0:T(8,128)(2,1)S(1)}, u32[]{:S(2)}, u32[]{:S(2)}) collective-permute-start(bf16[64,2048]{1,0:T(8,128)(2,1)S(1)} %constant_dynamic-update-slice_fusion.10), channel_id=1, source_target_pairs={{0,8},{4,12},{8,16},{12,20},{16,24},{20,28},{24,0},{28,4},{1,9},{5... | collective-permute-start | bytes 786440 | tf_op jit(solution)/shard_map/ppermute | solution.py:57
  110.3 10.7 %collective-permute-start.11 = (bf16[64,2048]{1,0:T(8,128)(2,1)S(1)}, bf16[64,2048]{1,0:T(8,128)(2,1)S(1)}, u32[]{:S(2)}, u32[]{:S(2)}) collective-permute-start(bf16[64,2048]{1,0:T(8,128)(2,1)S(1)} %constant_dynamic-update-slice_fusion.10), channel_id=1, source_target_pairs={{0,16},{4,20},{8,24},{12,28},{16,0},{20,4},{24,8},{28,12},{1,17},{... | collective-permute-start | bytes 786440 | tf_op jit(solution)/shard_map/ppermute | solution.py:57
  121.0 8.2 %collective-permute-start.12 = (bf16[64,2048]{1,0:T(8,128)(2,1)S(1)}, bf16[64,2048]{1,0:T(8,128)(2,1)S(1)}, u32[]{:S(2)}, u32[]{:S(2)}) collective-permute-start(bf16[64,2048]{1,0:T(8,128)(2,1)S(1)} %constant_dynamic-update-slice_fusion.10), channel_id=1, source_target_pairs={{0,24},{4,28},{8,0},{12,4},{16,8},{20,12},{24,16},{28,20},{1,25},{... | collective-permute-start | bytes 786440 | tf_op jit(solution)/shard_map/ppermute | solution.py:57
  129.3 11.6 %collective-permute-start.14 = (bf16[1024,512]{1,0:T(8,128)(2,1)}, bf16[1024,512]{1,0:T(8,128)(2,1)S(1)}, u32[]{:S(2)}, u32[]{:S(2)}) collective-permute-start(bf16[1024,512]{1,0:T(8,128)(2,1)} %bitcast.39), channel_id=1, source_target_pairs={{0,1},{1,0},{2,3},{3,2},{4,5},{5,4},{6,7},{7,6},{8,9},{9,8},{10,11... | collective-permute-start | bytes 3145736 | tf_op jit(solution)/shard_map/ppermute | solution.py:66
  129.4 31.4 %collective-permute-start.16 = (bf16[512,1024]{0,1:T(8,128)(2,1)S(1)}, bf16[512,1024]{0,1:T(8,128)(2,1)S(1)}, u32[]{:S(2)}, u32[]{:S(2)}) collective-permute-start(bf16[512,1024]{0,1:T(8,128)(2,1)S(1)} %bitcast.221), channel_id=1, source_target_pairs={{0,1},{1,0},{2,3},{3,2},{4,5},{5,4},{6,7},{7,6},{8,9},{9,8},{10,11... | collective-permute-start | bytes 3145736 | tf_op jit(solution)/shard_map/ppermute | solution.py:66
  131.0 14.9 %collective-permute-start.18 = (bf16[512,512]{1,0:T(8,128)(2,1)S(1)}, bf16[512,512]{1,0:T(8,128)(2,1)S(1)}, u32[]{:S(2)}, u32[]{:S(2)}) collective-permute-start(bf16[512,512]{1,0:T(8,128)(2,1)S(1)} %slice.79), channel_id=1, source_target_pairs={{0,2},{1,3},{2,0},{3,1},{4,6},{5,7},{6,4},{7,5},{8,10},{9,11},{10,... | collective-permute-start | bytes 1572872 | tf_op jit(solution)/shard_map/ppermute | solution.py:63
  132.7 14.9 %collective-permute-start.19 = (bf16[512,512]{1,0:T(8,128)(2,1)S(1)}, bf16[512,512]{1,0:T(8,128)(2,1)S(1)}, u32[]{:S(2)}, u32[]{:S(2)}) collective-permute-start(bf16[512,512]{1,0:T(8,128)(2,1)S(1)} %slice.80), channel_id=1, source_target_pairs={{0,4},{4,0},{8,12},{12,8},{16,20},{20,16},{24,28},{28,24},{1,5},{5... | collective-permute-start | bytes 1572872 | tf_op jit(solution)/shard_map/ppermute | solution.py:60
  134.4 21.8 %collective-permute-start.26 = (bf16[256,1024]{0,1:T(8,128)(2,1)S(1)}, bf16[256,1024]{0,1:T(8,128)(2,1)S(1)}, u32[]{:S(2)}, u32[]{:S(2)}) collective-permute-start(bf16[256,1024]{0,1:T(8,128)(2,1)S(1)} %slice.81), channel_id=1, source_target_pairs={{0,2},{1,3},{2,0},{3,1},{4,6},{5,7},{6,4},{7,5},{8,10},{9,11},{10,... | collective-permute-start | bytes 1572872 | tf_op jit(solution)/shard_map/ppermute | solution.py:63
  140.8 16.8 %collective-permute-start.27 = (bf16[256,1024]{0,1:T(8,128)(2,1)S(1)}, bf16[256,1024]{0,1:T(8,128)(2,1)S(1)}, u32[]{:S(2)}, u32[]{:S(2)}) collective-permute-start(bf16[256,1024]{0,1:T(8,128)(2,1)S(1)} %slice.82), channel_id=1, source_target_pairs={{0,4},{4,0},{8,12},{12,8},{16,20},{20,16},{24,28},{28,24},{1,5},{5... | collective-permute-start | bytes 1572872 | tf_op jit(solution)/shard_map/ppermute | solution.py:60
  145.9 17.7 %collective-permute-start.21 = (bf16[1024,512]{1,0:T(8,128)(2,1)}, bf16[1024,512]{1,0:T(8,128)(2,1)S(1)}, u32[]{:S(2)}, u32[]{:S(2)}) collective-permute-start(bf16[1024,512]{1,0:T(8,128)(2,1)} %collective-permute-done.17), channel_id=1, source_target_pairs={{0,1},{1,0},{2,3},{3,2},{4,5},{5,4},{6,7},{7,6},{8,9},{9,8},{10,11... | collective-permute-start | bytes 3145736 | tf_op jit(solution)/shard_map/ppermute | solution.py:66
  147.6 12.2 %collective-permute-start.15 = (bf16[1024,512]{1,0:T(8,128)(2,1)}, bf16[1024,512]{1,0:T(8,128)(2,1)S(1)}, u32[]{:S(2)}, u32[]{:S(2)}) collective-permute-start(bf16[1024,512]{1,0:T(8,128)(2,1)} %collective-permute-done.13), channel_id=1, source_target_pairs={{0,1},{1,0},{2,3},{3,2},{4,5},{5,4},{6,7},{7,6},{8,9},{9,8},{10,11... | collective-permute-start | bytes 3145736 | tf_op jit(solution)/shard_map/ppermute | solution.py:66
  156.2 9.2 %collective-permute-start.25 = (bf16[512,1024]{0,1:T(8,128)(2,1)S(1)}, bf16[512,1024]{0,1:T(8,128)(2,1)S(1)}, u32[]{:S(2)}, u32[]{:S(2)}) collective-permute-start(bf16[512,1024]{0,1:T(8,128)(2,1)S(1)} %collective-permute-done.24), channel_id=1, source_target_pairs={{0,1},{1,0},{2,3},{3,2},{4,5},{5,4},{6,7},{7,6},{8,9},{9,8},{10,11... | collective-permute-start | bytes 3145736 | tf_op jit(solution)/shard_map/ppermute | solution.py:66
  157.6 5.5 %collective-permute-start.22 = (bf16[1024,512]{1,0:T(8,128)(2,1)S(1)}, bf16[1024,512]{1,0:T(8,128)(2,1)S(1)}, u32[]{:S(2)}, u32[]{:S(2)}) collective-permute-start(bf16[1024,512]{1,0:T(8,128)(2,1)S(1)} %constant_dynamic-update-slice_fusion.12), channel_id=1, source_target_pairs={{0,1},{1,0},{2,3},{3,2},{4,5},{5,4},{6,7},{7,6},{8,9},{9,8},{10,11... | collective-permute-start | bytes 3145736 | tf_op jit(solution)/shard_map/ppermute | solution.py:66
  159.8 5.0 %collective-permute-start.23 = (bf16[512,1024]{0,1:T(8,128)(2,1)}, bf16[512,1024]{0,1:T(8,128)(2,1)S(1)}, u32[]{:S(2)}, u32[]{:S(2)}) collective-permute-start(bf16[512,1024]{0,1:T(8,128)(2,1)} %collective-permute-done.20), channel_id=1, source_target_pairs={{0,1},{1,0},{2,3},{3,2},{4,5},{5,4},{6,7},{7,6},{8,9},{9,8},{10,11... | collective-permute-start | bytes 3145736 | tf_op jit(solution)/shard_map/ppermute | solution.py:66
  160.8 3.5 %collective-permute-start.28 = (bf16[512,1024]{0,1:T(8,128)(2,1)S(1)}, bf16[512,1024]{0,1:T(8,128)(2,1)S(1)}, u32[]{:S(2)}, u32[]{:S(2)}) collective-permute-start(bf16[512,1024]{0,1:T(8,128)(2,1)S(1)} %constant_dynamic-update-slice_fusion.14), channel_id=1, source_target_pairs={{0,1},{1,0},{2,3},{3,2},{4,5},{5,4},{6,7},{7,6},{8,9},{9,8},{10,11... | collective-permute-start | bytes 3145736 | tf_op jit(solution)/shard_map/ppermute | solution.py:66
  166.0 9.4 %collective-permute-start.29 = (bf16[64,2048]{1,0:T(8,128)(2,1)S(1)}, bf16[64,2048]{1,0:T(8,128)(2,1)S(1)}, u32[]{:S(2)}, u32[]{:S(2)}) collective-permute-start(bf16[64,2048]{1,0:T(8,128)(2,1)S(1)} %get-tuple-element.11), channel_id=1, source_target_pairs={{0,24},{4,28},{8,0},{12,4},{16,8},{20,12},{24,16},{28,20},{1,25},{... | collective-permute-start | bytes 786440 | tf_op jit(solution)/shard_map/ppermute | solution.py:57
  168.2 22.9 %collective-permute-start.30 = (bf16[64,2048]{1,0:T(8,128)(2,1)S(1)}, bf16[64,2048]{1,0:T(8,128)(2,1)}, u32[]{:S(2)}, u32[]{:S(2)}) collective-permute-start(bf16[64,2048]{1,0:T(8,128)(2,1)S(1)} %get-tuple-element.13), channel_id=1, source_target_pairs={{0,16},{4,20},{8,24},{12,28},{16,0},{20,4},{24,8},{28,12},{1,17},{... | collective-permute-start | bytes 786440 | tf_op jit(solution)/shard_map/ppermute | solution.py:57
  168.2 22.9 %collective-permute-start.31 = (bf16[64,2048]{1,0:T(8,128)(2,1)S(1)}, bf16[64,2048]{1,0:T(8,128)(2,1)}, u32[]{:S(2)}, u32[]{:S(2)}) collective-permute-start(bf16[64,2048]{1,0:T(8,128)(2,1)S(1)} %get-tuple-element.12), channel_id=1, source_target_pairs={{0,8},{4,12},{8,16},{12,20},{16,24},{20,28},{24,0},{28,4},{1,9},{5... | collective-permute-start | bytes 786440 | tf_op jit(solution)/shard_map/ppermute | solution.py:57
